TPU v7x, 32 devices: a whole 2x2x4 slice. The times are simulated.
32 devices in a mesh: sp: 16 (over z, y, x), tp: 2 (over core).
Axes of the slice: x: 2, y: 2, z: 4, core: 2. Of those that a mesh axis runs over, the one named last changes fastest.
Arguments:
- conv_value: bfloat16 [4096, 1024], P('sp', 'tp'), may hold values from -6 to 6
- conv_gate: bfloat16 [4096, 1024], P('sp', 'tp'), may hold values from -6 to 6
- taps: bfloat16 [31, 1024], P(None, 'tp'), may hold values from -1 to 1
- doc_ids: int32 [4096], P('sp'), may hold values from 0 to 3, never falling along the last dimension, each value on 1 to 2048 neighbouring positions
- gn_gain: float32 [1024], P('tp'), may hold values from 0.1 to 1.9
- gn_shift: float32 [1024], P('tp'), may hold values from -3 to 3
- conv_out: bfloat16 [1024, 2048], replicated, may hold values from -0.1875 to 0.1875
- residual: bfloat16 [4096, 2048], P(('sp', 'tp')), may hold values from -6 to 6
- norm_gain: float32 [2048], replicated, may hold values from 0.1 to 1.9
- routes: int32 [4096, 2], P(('sp', 'tp')), may hold values from 0 to 31, as said below
- route_weight: float32 [4096, 2], P(('sp', 'tp')), may hold values from 0.3 to 1.2
- expert_gate: bfloat16 [32, 2048, 512], P(('sp', 'tp')), may hold values from -0.125 to 0.125
- expert_up: bfloat16 [32, 2048, 512], P(('sp', 'tp')), may hold values from -0.125 to 0.125
- expert_down: bfloat16 [32, 512, 2048], P(('sp', 'tp')), may hold values from -0.25 to 0.25
- shared_gate: bfloat16 [2048, 512], replicated, may hold values from -0.125 to 0.125
- shared_up: bfloat16 [2048, 512], replicated, may hold values from -0.125 to 0.125
- shared_down: bfloat16 [512, 2048], replicated, may hold values from -0.25 to 0.25
Outputs:
- layer_out: bfloat16 [4096, 2048], P(('sp', 'tp'))
Inputs may be any that keep to these rules, and one draw needn't show every extreme that they name: `routes`: each row names 2 different experts. The rows of one device name each expert at most 16 times, and one expert, the same for every device, exactly 16 times. `doc_ids`: numbers never fall from one position to the next.
All inputs are finite; a program needn't handle non-finite values.
Results may differ from a plain program's by a relative error of at most 0.014.
Values may be sent and summed in bfloat16 or wider, within the bound.
A program may use at most 128 MiB of HBM per device.

v0:
```python
import jax
import jax.numpy as jnp
from jax import lax
from jax.sharding import PartitionSpec as P

GROUPS = 8
epsilon = 1e-06


def from_behind(x, axis, by):
    peers = lax.axis_size(axis)
    pairs = [(i, i + by) for i in range(peers) if 0 <= i + by < peers]
    return lax.ppermute(x, axis, pairs)


def per_device(
    conv_value,
    conv_gate,
    taps,
    doc_ids,
    gn_gain,
    gn_shift,
    conv_out,
    residual,
    norm_gain,
    routes,
    route_weight,
    expert_gate,
    expert_up,
    expert_down,
    shared_gate,
    shared_up,
    shared_down,
):
    position_count, channel_count = conv_value.shape
    kernel_width = taps.shape[0]
    model_width = residual.shape[1]
    glu_out = (
        conv_value.astype(jnp.float32) * jax.nn.sigmoid(conv_gate.astype(jnp.float32))
    ).astype(jnp.bfloat16)
    rim_start = position_count - kernel_width + 1
    edge_glu, edge_ids = from_behind((glu_out[rim_start:], doc_ids[rim_start:]), "sp", 1)
    longer_glu = jnp.concatenate([edge_glu, glu_out], axis=0)
    longer_ids = jnp.concatenate([edge_ids, doc_ids], axis=0)
    conv_sum = jnp.zeros((position_count, channel_count), jnp.float32)
    for offset in range(kernel_width):
        same_doc = (longer_ids[offset : offset + position_count] == doc_ids)[:, None]
        tap_term = taps[offset].astype(jnp.float32)[None, :] * longer_glu[
            offset : offset + position_count
        ].astype(jnp.float32)
        conv_sum = conv_sum + jnp.where(same_doc, tap_term, 0.0)
    core_split = lax.axis_size("tp")
    groups_here = GROUPS // core_split
    grouped = conv_sum.reshape(position_count, groups_here, channel_count // groups_here)
    group_mean = jnp.mean(grouped, axis=-1, keepdims=True)
    centered = grouped - group_mean
    group_var = jnp.mean(centered * centered, axis=-1, keepdims=True)
    normalized = (centered * lax.rsqrt(group_var + epsilon)).reshape(position_count, channel_count)
    conv_act = jax.nn.silu(normalized * gn_gain + gn_shift).astype(jnp.bfloat16)
    token_rows = lax.all_to_all(conv_act, "tp", split_axis=0, concat_axis=1, tiled=True)
    projected = jnp.dot(token_rows, conv_out, preferred_element_type=jnp.float32)
    stream = (residual.astype(jnp.float32) + projected).astype(jnp.bfloat16)
    stream_wide = stream.astype(jnp.float32)
    normed = (
        stream_wide
        * lax.rsqrt(jnp.mean(stream_wide * stream_wide, axis=-1, keepdims=True) + epsilon)
        * norm_gain
    ).astype(jnp.bfloat16)
    token_count, top_count = routes.shape
    sequence_split = lax.axis_size("sp")
    device_count = sequence_split * core_split
    local_experts = expert_gate.shape[0]
    experts = local_experts * device_count
    capacity = 2 * token_count * top_count // experts
    flat_routes = routes.reshape(-1)
    onehot = (flat_routes[:, None] == jnp.arange(experts, dtype=jnp.int32)[None, :]).astype(
        jnp.int32
    )
    slot_index = jnp.sum(jnp.cumsum(onehot, axis=0) * onehot, axis=1) - 1
    target = flat_routes * capacity + slot_index
    source = (
        jnp.full((experts * capacity,), token_count, jnp.int32)
        .at[target]
        .set(jnp.arange(token_count * top_count, dtype=jnp.int32) // top_count)
    )
    padded_rows = jnp.concatenate([normed, jnp.zeros((1, model_width), normed.dtype)], axis=0)
    outgoing = padded_rows[source]
    shared_hidden = (
        jax.nn.silu(jnp.dot(normed, shared_gate, preferred_element_type=jnp.float32))
        * jnp.dot(normed, shared_up, preferred_element_type=jnp.float32)
    ).astype(jnp.bfloat16)
    shared_out = jnp.dot(shared_hidden, shared_down, preferred_element_type=jnp.float32)
    parcel = outgoing.reshape(device_count, local_experts, capacity, model_width)
    arrived = lax.all_to_all(parcel, ("sp", "tp"), split_axis=0, concat_axis=0, tiled=True)
    expert_rows = arrived[:, 0].reshape(-1, model_width)
    gate_part = jnp.dot(expert_rows, expert_gate[0], preferred_element_type=jnp.float32)
    up_part = jnp.dot(expert_rows, expert_up[0], preferred_element_type=jnp.float32)
    hidden = (jax.nn.silu(gate_part) * up_part).astype(jnp.bfloat16)
    result = jnp.dot(hidden, expert_down[0], preferred_element_type=jnp.float32).astype(
        jnp.bfloat16
    )
    results = [result.reshape(arrived.shape[0], arrived.shape[2], model_width)]
    returned = lax.all_to_all(
        jnp.stack(results, axis=1), ("sp", "tp"), split_axis=0, concat_axis=0, tiled=True
    )
    picked = returned.reshape(experts * capacity, model_width)[target].reshape(
        token_count, top_count, model_width
    )
    routed = jnp.zeros((token_count, model_width), jnp.float32)
    for route_index in range(top_count):
        routed = routed + route_weight[:, route_index, None] * picked[:, route_index].astype(
            jnp.float32
        )
    return (stream_wide + shared_out + routed).astype(jnp.bfloat16)


def solution(mesh):
    return jax.shard_map(
        per_device,
        mesh=mesh,
        in_specs=(
            P("sp", "tp"),
            P("sp", "tp"),
            P(None, "tp"),
            P("sp"),
            P("tp"),
            P("tp"),
            P(),
            P(("sp", "tp"), None),
            P(),
            P(("sp", "tp"), None),
            P(("sp", "tp"), None),
            P(("sp", "tp"), None, None),
            P(("sp", "tp"), None, None),
            P(("sp", "tp"), None, None),
            P(),
            P(),
            P(),
        ),
        out_specs=P(("sp", "tp"), None),
        check_vma=False,
    )
```

profile of v0, /device:TPU:0, one launch (start us, length us, event | category | flops | bytes accessed | tf_op | source)
XLA Modules:
  0.0 168.0 jit_solution(8082973115691364182)
XLA Ops:
  0.0 0.9 slice.297
  0.9 4.9 %collective-permute-start = (s32[30]{0:T(128)S(1)}, s32[30]{0:T(128)S(1)}, u32[]{:S(2)}, u32[]{:S(2)}) collective-permute-start(s32[30]{0:T(128)S(1)} %slice.297), channel_id=1, source_target_pairs={{0,2},{2,4},{4,6},{6,8},{8,10},{10,12},{12,14},{14,16},{16,18},{18... | collective-permute-start | bytes 368 | tf_op jit(solution)/shard_map/ppermute | solution.py:13
  5.8 1.2 multiply_convert_fusion.2
  7.0 3.4 %collective-permute-start.1 = (bf16[30,512]{1,0:T(8,128)(2,1)S(1)}, bf16[30,512]{1,0:T(8,128)(2,1)S(1)}, u32[]{:S(2)}, u32[]{:S(2)}) collective-permute-start(bf16[30,512]{1,0:T(8,128)(2,1)S(1)} %slice.400), channel_id=1, source_target_pairs={{0,2},{2,4},{4,6},{6,8},{8,10},{10,12},{12,14},{14,16},{16,18},{18... | collective-permute-start | bytes 92168 | tf_op jit(solution)/shard_map/ppermute | solution.py:13
  10.4 1.0 slice_convert_fusion.30
  11.4 1.0 slice_convert_fusion.29
  12.4 0.8 copy.33
  13.5 0.7 broadcast_multiply_fusion.1
  14.2 0.6 reduce-window.6
  15.4 1.4 scatter_custom_fusion
  16.8 0.8 pad_add_fusion
  17.6 0.8 slice_compare_fusion.29
  18.4 0.8 slice_compare_fusion.28
  19.1 4.0 %multiply_add_fusion = f32[256,512]{1,0:T(8,128)S(1)} fusion(bf16[256,512]{1,0:T(8,128)(2,1)S(1)} %multiply_convert_fusion.2, bf16[30,512]{1,0:T(8,128)(2,1)S(1)} %collective-permute-done.1, f32[512]{0:T(512)S(1)} %bitcast.151, f32[512]{0:T(512)S(1)} %bitcast.152, f32[512]{0:T(512)S(1)} %bitcast.123, f32[512]{0:T(512)S(1)} %bitcast.124, ...), kind=kLoop, calls=%fused_computation.62 | loop fusion | flops 27787264 | bytes 888320 | tf_op jit(solution)/shard_map/add | solution.py:51
  23.4 0.3 reduce_sum.36
  23.8 0.6 multiply_reduce_fusion.1
  24.8 0.3 sub.25
  25.3 3.9 %all_to_all.29 = bf16[2,128,512]{2,1,0:T(8,128)(2,1)S(1)} all-to-all(bf16[2,128,512]{2,1,0:T(8,128)(2,1)S(1)} %bitcast.119), channel_id=1, replica_groups=mesh['sp'=16,'tp'=2] {'tp'}, dimensions={0} | all-to-all | bytes 524288 | tf_op jit(solution)/shard_map/all_to_all | solution.py:60
  29.5 3.0 %multiply_reduce_fusion = (f32[128]{0:T(128)S(1)}, f32[128,2048]{1,0:T(8,128)S(1)}) fusion(bf16[128,1024]{0,1:T(8,128)(2,1)S(1)} %bitcast.120, bf16[1024,2048]{1,0:T(8,128)(2,1)} %param.23, bf16[128,2048]{1,0:T(8,128)(2,1)S(1)} %copy-done.4), kind=kOutput, calls=%fused_computation.52 | convolution fusion | flops 538443648 | bytes 6029824 | tf_op jit(solution)/shard_map/dot_general | solution.py:61
  32.5 1.0 copy-done.2
  33.7 3.3 %gather_fusion = bf16[512,2048]{1,0:T(8,128)(2,1)} fusion(bf16[129,2048]{1,0:T(8,128)(2,1)S(1)} %concatenate.11, s32[1024]{0:T(1024)S(1)} %pad_clamp_fusion.1), kind=kCustom, calls=%fused_computation | custom fusion | bytes 4196352 | tf_op jit(solution)/shard_map/gather | solution.py:87
  37.1 53.6 %all_to_all.30 = bf16[32,1,16,2048]{3,2,1,0:T(8,128)(2,1)S(1)} all-to-all(bf16[32,1,16,2048]{3,2,1,0:T(8,128)(2,1)} %bitcast.113), channel_id=1, replica_groups=mesh['sp'=16,'tp'=2] {'sp','tp'}, dimensions={0} | all-to-all | bytes 4194304 | tf_op jit(solution)/shard_map/all_to_all | solution.py:94
  90.6 1.3 copy-done.3
  91.9 2.3 %fusion.7 = f32[512,512]{1,0:T(8,128)} fusion(bf16[512,2048]{1,0:T(8,128)(2,1)S(1)} %bitcast.117, bf16[1,2048,512]{2,1,0:T(8,128)(2,1)S(1)} %copy-done.9), kind=kOutput, calls=%fused_computation.42 | convolution fusion | flops 1073741824 | bytes 5242880 | tf_op jit(solution)/shard_map/dot_general | solution.py:96
  94.2 6.3 %convolution_convert_fusion = bf16[512,2048]{1,0:T(8,128)(2,1)} fusion(bf16[1,512,2048]{2,1,0:T(8,128)(2,1)S(1)} %copy-done, bf16[512,2048]{1,0:T(8,128)(2,1)} %bitcast.118, bf16[1,2048,512]{2,1,0:T(8,128)(2,1)} %param.29, f32[512,512]{1,0:T(8,128)} %fusion.7), kind=kOutput, calls=%fused_computation.3 | convolution fusion | flops 2150105088 | bytes 9437184 | tf_op jit(solution)/shard_map/dot_general | solution.py:99
  100.5 4.0 %all-to-all-start.2 = ((bf16[32,1,16,2048]{3,2,1,0:T(8,128)(2,1)}), bf16[32,1,16,2048]{3,2,1,0:T(8,128)(2,1)}, u32[]{:S(2)}, u32[]{:S(2)}) async-start(bf16[32,1,16,2048]{3,2,1,0:T(8,128)(2,1)} %bitcast.116), calls=%async_computation.2 | async-start | bytes 4194304 | tf_op jit(solution)/shard_map/all_to_all | solution.py:103
  104.5 2.0 %fusion.65 = f32[128,512]{1,0:T(8,128)S(1)} fusion(bf16[128,2048]{1,0:T(8,128)(2,1)S(1)} %multiply_convert_fusion, bf16[2048,512]{1,0:T(8,128)(2,1)} %param.31), kind=kOutput, calls=%fused_computation.198 | convolution fusion | flops 268435456 | bytes 2883584 | tf_op jit(solution)/shard_map/dot_general | solution.py:89
  106.5 46.6 %all-to-all-done.2 = bf16[32,1,16,2048]{3,2,1,0:T(8,128)(2,1)} async-done(((bf16[32,1,16,2048]{3,2,1,0:T(8,128)(2,1)}), bf16[32,1,16,2048]{3,2,1,0:T(8,128)(2,1)}, u32[]{:S(2)}, u32[]{:S(2)}) %all-to-all-start.2) | async-done | bytes 2097184 | tf_op jit(solution)/shard_map/all_to_all | solution.py:103
  153.1 5.2 %gather_fusion.1 = bf16[256,2048]{1,0:T(8,128)(2,1)} fusion(bf16[512,2048]{1,0:T(8,128)(2,1)} %bitcast.46, s32[1024]{0:T(1024)S(1)} %pad_clamp_fusion), kind=kCustom, calls=%fused_computation.1 | custom fusion | bytes 2098176 | tf_op jit(solution)/shard_map/gather | solution.py:106
  158.3 1.7 %reshape.130 = bf16[128,2,2048]{2,1,0:T(2,128)(2,1)S(1)} reshape(bf16[256,2048]{1,0:T(8,128)(2,1)} %gather_fusion.1) | data formatting | bytes 2097152 | tf_op jit(solution)/shard_map/reshape | solution.py:106
  160.1 2.5 %fusion.64 = (bf16[128,1,2048]{2,1,0:T(2,128)(2,1)}, bf16[128,1,2048]{2,1,0:T(2,128)(2,1)}) fusion(bf16[128,2,2048]{2,1,0:T(2,128)(2,1)S(1)} %reshape.130), kind=kLoop, calls=%fused_computation.197 | loop fusion | bytes 2097152 | tf_op jit(solution)/shard_map/slice | solution.py:111
  162.6 5.4 %fusion.3 = bf16[128,2048]{1,0:T(8,128)(2,1)} fusion(f32[128,2048]{1,0:T(8,128)} %copy-done.2, bf16[512,2048]{1,0:T(8,128)(2,1)} %param.33, bf16[128,2048]{1,0:T(8,128)(2,1)} %copy-done.1, bf16[2048,512]{1,0:T(8,128)(2,1)} %param.32, bf16[128,1,2048]{2,1,0:T(2,128)(2,1)} %get-tuple-element.6, bf16[128,1,2048]{2,1,0:T(2,128)(2,1)} %get-tuple-element.5, ...), kind=kOutput, calls=%fused_computation.38 | convolution fusion | flops 539361280 | bytes 7603200 | tf_op jit(solution)/shard_map/dot_general | solution.py:92
  (46 shorter events, 2.1 us)
Async XLA Ops:
  0.0 94.2 %copy-start = (bf16[1,512,2048]{2,1,0:T(8,128)(2,1)S(1)}, bf16[1,512,2048]{2,1,0:T(8,128)(2,1)}, u32[]{:S(2)}) copy-start(bf16[1,512,2048]{2,1,0:T(8,128)(2,1)} %param.30) | copy-start | bytes 6291460
  0.9 15.9 %collective-permute-start = (s32[30]{0:T(128)S(1)}, s32[30]{0:T(128)S(1)}, u32[]{:S(2)}, u32[]{:S(2)}) collective-permute-start(s32[30]{0:T(128)S(1)} %slice.297), channel_id=1, source_target_pairs={{0,2},{2,4},{4,6},{6,8},{8,10},{10,12},{12,14},{14,16},{16,18},{18... | collective-permute-start | bytes 368 | tf_op jit(solution)/shard_map/ppermute | solution.py:13
  7.0 12.2 %collective-permute-start.1 = (bf16[30,512]{1,0:T(8,128)(2,1)S(1)}, bf16[30,512]{1,0:T(8,128)(2,1)S(1)}, u32[]{:S(2)}, u32[]{:S(2)}) collective-permute-start(bf16[30,512]{1,0:T(8,128)(2,1)S(1)} %slice.400), channel_id=1, source_target_pairs={{0,2},{2,4},{4,6},{6,8},{8,10},{10,12},{12,14},{14,16},{16,18},{18... | collective-permute-start | bytes 92168 | tf_op jit(solution)/shard_map/ppermute | solution.py:13
  23.2 1.9 %copy-start.6 = (f32[512]{0:T(512)S(1)}, f32[512]{0:T(512)}, u32[]{:S(2)}) copy-start(f32[512]{0:T(512)} %param.22) | copy-start | bytes 6148
  23.2 1.9 %copy-start.7 = (f32[512]{0:T(512)S(1)}, f32[512]{0:T(512)}, u32[]{:S(2)}) copy-start(f32[512]{0:T(512)} %param.21) | copy-start | bytes 6148
  24.4 5.0 %copy-start.4 = (bf16[128,2048]{1,0:T(8,128)(2,1)S(1)}, bf16[128,2048]{1,0:T(8,128)(2,1)}, u32[]{:S(2)}) copy-start(bf16[128,2048]{1,0:T(8,128)(2,1)} %param.24) | copy-start | bytes 1572868
  29.5 4.0 %copy-start.5 = (f32[2048]{0:T(1024)S(1)}, f32[2048]{0:T(1024)}, u32[]{:S(2)}) copy-start(f32[2048]{0:T(1024)} %param.25) | copy-start | bytes 24580
  32.5 1.0 copy-start.2
  33.6 70.8 %copy-start.1 = (bf16[128,2048]{1,0:T(8,128)(2,1)}, bf16[128,2048]{1,0:T(8,128)(2,1)S(1)}, u32[]{:S(2)}) copy-start(bf16[128,2048]{1,0:T(8,128)(2,1)S(1)} %multiply_convert_fusion) | copy-start | bytes 1572868
  37.1 54.9 %copy-start.9 = (bf16[1,2048,512]{2,1,0:T(8,128)(2,1)S(1)}, bf16[1,2048,512]{2,1,0:T(8,128)(2,1)}, u32[]{:S(2)}) copy-start(bf16[1,2048,512]{2,1,0:T(8,128)(2,1)} %param.28) | copy-start | bytes 6291460
  90.6 1.3 copy-start.3
  100.5 4.0 %copy-start.8 = (f32[128,2]{0,1:T(2,128)S(1)}, f32[128,2]{0,1:T(2,128)}, u32[]{:S(2)}) copy-start(f32[128,2]{0,1:T(2,128)} %param.27) | copy-start | bytes 3076
  100.5 52.6 %all-to-all-start.2 = ((bf16[32,1,16,2048]{3,2,1,0:T(8,128)(2,1)}), bf16[32,1,16,2048]{3,2,1,0:T(8,128)(2,1)}, u32[]{:S(2)}, u32[]{:S(2)}) async-start(bf16[32,1,16,2048]{3,2,1,0:T(8,128)(2,1)} %bitcast.116), calls=%async_computation.2 | async-start | bytes 4194304 | tf_op jit(solution)/shard_map/all_to_all | solution.py:103
where the time goes:
time: 169 us; the launch traced here: 168 us
  blocking collectives  57.5 us (34%)
  waiting for transfers between devices  46.6 us (28%)
  local copies, waits for them, and re-layouts  20 us (12%)
  matrix products  19 us (11%)
  other arithmetic  12.3 us (7%)
  starting transfers between devices  12.2 us (7%)
    all_to_all x1, blocking collectives, per_device(): lax.all_to_all(parcel, ('sp', 'tp'), split_axis=0, concat_axis=0, tiled=T...  53.6 us
    all_to_all x1, waiting for transfers between devices, per_device(): lax.all_to_all(jnp.stack(results, axis=1), ('sp', 'tp'), split_axis=0, co...  46.6 us
    ppermute x2, starting transfers between devices, from_behind(): return lax.ppermute(x, axis, pairs)  8.26 us
    dot_general x1, matrix products, per_device(): jnp.dot(hidden, expert_down[0], preferred_element_type=jnp.float32)  6.28 us
    dot_general x1, matrix products, per_device(): jnp.dot(shared_hidden, shared_down, preferred_element_type=jnp.float32)  5.43 us
    gather x1, local copies, waits for them, and re-layouts, per_device(): returned.reshape(experts * capacity, model_width)[target]  5.21 us
    add x1, other arithmetic, per_device(): conv_sum = conv_sum + jnp.where(same_doc, tap_term, 0.0)  4.03 us
    all_to_all x1, starting transfers between devices, per_device(): lax.all_to_all(jnp.stack(results, axis=1), ('sp', 'tp'), split_axis=0, co...  3.96 us
  transfers between devices with their start and end apart: 3, of which 1 were waited for; matrix products, arithmetic and copies ran while one was open for 7% of the time, Pallas kernels for 0%

commit v1 on v0

--- a/solution.py
+++ b/solution.py
@@ -57,7 +57,10 @@
     group_var = jnp.mean(centered * centered, axis=-1, keepdims=True)
     normalized = (centered * lax.rsqrt(group_var + epsilon)).reshape(position_count, channel_count)
     conv_act = jax.nn.silu(normalized * gn_gain + gn_shift).astype(jnp.bfloat16)
-    token_rows = lax.all_to_all(conv_act, "tp", split_axis=0, concat_axis=1, tiled=True)
+    token_rows = jnp.concatenate(
+        lax.all_to_all(jnp.stack(jnp.split(conv_act, lax.axis_size("tp"), axis=0)), "tp", 0, 0),
+        axis=1,
+    )
     projected = jnp.dot(token_rows, conv_out, preferred_element_type=jnp.float32)
     stream = (residual.astype(jnp.float32) + projected).astype(jnp.bfloat16)
     stream_wide = stream.astype(jnp.float32)

time: 169 us -> 166 us (0.982)
  other arithmetic: 12.3 us -> 8.06 us
    reduce_sum x1, other arithmetic: 0.34 us -> 6.33 us  [per_device(): group_mean = jnp.mean(grouped, axis=-1, keepdims=True)]
    add x1 -> x0, other arithmetic: 4.03 us -> none  [per_device(): conv_sum = conv_sum + jnp.where(same_doc, tap_term, 0.0)]
    mul x2, other arithmetic: 2.02 us -> 0.05 us  [per_device(): taps[offset].astype(jnp.float32)[None, :]]
    unnamed x21 -> x29, local copies, waits for them, and re-layouts: 3.09 us -> 4.61 us
  transfers between devices with their start and end apart: 3 -> 3, of which waited for: 1 -> 1; matrix products, arithmetic and copies ran while one was open for 7% -> 5% of each run, Pallas kernels for 0% -> 0%
where the time goes in v1:
time: 166 us; the launch traced here: 165 us
  blocking collectives  58.3 us (35%)
  waiting for transfers between devices  46.6 us (28%)
  local copies, waits for them, and re-layouts  20.5 us (12%)
  matrix products  19 us (11%)
  starting transfers between devices  12.2 us (7%)
  other arithmetic  8.06 us (5%)
    all_to_all x1, blocking collectives, per_device(): lax.all_to_all(parcel, ('sp', 'tp'), split_axis=0, concat_axis=0, tiled=T...  54.3 us
    all_to_all x1, waiting for transfers between devices, per_device(): lax.all_to_all(jnp.stack(results, axis=1), ('sp', 'tp'), split_axis=0, co...  46.6 us
    ppermute x2, starting transfers between devices, from_behind(): return lax.ppermute(x, axis, pairs)  8.27 us
    reduce_sum x1, other arithmetic, per_device(): group_mean = jnp.mean(grouped, axis=-1, keepdims=True)  6.33 us
    dot_general x1, matrix products, per_device(): jnp.dot(hidden, expert_down[0], preferred_element_type=jnp.float32)  6.25 us
    dot_general x1, matrix products, per_device(): jnp.dot(shared_hidden, shared_down, preferred_element_type=jnp.float32)  5.43 us
    gather x1, local copies, waits for them, and re-layouts, per_device(): returned.reshape(experts * capacity, model_width)[target]  5.19 us
    unnamed x29, local copies, waits for them, and re-layouts  4.61 us
  transfers between devices with their start and end apart: 3, of which 1 were waited for; matrix products, arithmetic and copies ran while one was open for 5% of the time, Pallas kernels for 0%

profile of v1, /device:TPU:0, one launch (start us, length us, event | category | flops | bytes accessed | tf_op | source)
XLA Modules:
  0.0 165.1 jit_solution(3022685406008928230)
XLA Ops:
  0.0 0.9 slice.297
  0.9 4.9 %collective-permute-start = (s32[30]{0:T(128)S(1)}, s32[30]{0:T(128)S(1)}, u32[]{:S(2)}, u32[]{:S(2)}) collective-permute-start(s32[30]{0:T(128)S(1)} %slice.297), channel_id=1, source_target_pairs={{0,2},{2,4},{4,6},{6,8},{8,10},{10,12},{12,14},{14,16},{16,18},{18... | collective-permute-start | bytes 368 | tf_op jit(solution)/shard_map/ppermute | solution.py:13
  5.8 1.1 copy.26
  6.9 1.1 copy.27
  8.0 0.2 multiply_convert_fusion.2
  8.3 3.4 %collective-permute-start.1 = (bf16[30,512]{0,1:T(8,128)(2,1)S(1)}, bf16[30,512]{0,1:T(8,128)(2,1)S(1)}, u32[]{:S(2)}, u32[]{:S(2)}) collective-permute-start(bf16[30,512]{0,1:T(8,128)(2,1)S(1)} %slice.400), channel_id=1, source_target_pairs={{0,2},{2,4},{4,6},{6,8},{8,10},{10,12},{12,14},{14,16},{16,18},{18... | collective-permute-start | bytes 92168 | tf_op jit(solution)/shard_map/ppermute | solution.py:13
  11.8 0.1 copy.29
  11.9 0.1 eq.149
  12.0 0.1 eq.145
  12.2 0.6 reduce-window.6
  12.8 0.2 slice_reduce_fusion
  13.1 0.1 copy.28
  13.2 0.1 mul.647
  13.4 1.4 scatter_custom_fusion
  15.1 6.3 %bitcast_reduce_fusion = (f32[256,4]{0,1:T(4,128)S(1)}, f32[256,512]{0,1:T(8,128)S(1)}) fusion(bf16[256,512]{0,1:T(8,128)(2,1)S(1)} %multiply_convert_fusion.2, f32[512]{0:T(512)S(1)} %bitcast.156, bf16[30,512]{0,1:T(8,128)(2,1)S(1)} %collective-permute-done.1, f32[512]{0:T(512)S(1)} %bitcast.157, pred[256]{0:T(512)(128)(4,1)S(1)} %get-tuple-element.70, ...), kind=kLoop, calls=%fused_computation.89 | loop fusion | flops 27917312 | bytes 892416 | tf_op jit(solution)/shard_map/reduce_sum | solution.py:55
  21.6 0.2 multiply_convert_fusion.1
  21.9 3.9 %all_to_all.15 = bf16[2,128,512]{1,2,0:T(8,128)(2,1)S(1)} all-to-all(bf16[2,128,512]{1,2,0:T(8,128)(2,1)S(1)} %pad_maximum_fusion.1), channel_id=1, replica_groups=mesh['sp'=16,'tp'=2] {'tp'}, dimensions={0} | all-to-all | bytes 524288 | tf_op jit(solution)/shard_map/all_to_all | solution.py:61
  25.9 3.0 %multiply_reduce_fusion = (f32[128]{0:T(128)S(1)}, f32[128,2048]{1,0:T(8,128)S(1)}) fusion(bf16[128,1024]{0,1:T(8,128)(2,1)S(1)} %bitcast.126, bf16[1024,2048]{1,0:T(8,128)(2,1)} %param.23, bf16[128,2048]{1,0:T(8,128)(2,1)S(1)} %copy-done.4), kind=kOutput, calls=%fused_computation.52 | convolution fusion | flops 538443648 | bytes 6029824 | tf_op jit(solution)/shard_map/dot_general | solution.py:64
  28.9 1.0 copy-done.2
  29.9 0.2 multiply_convert_fusion
  30.1 3.3 %gather_fusion = bf16[512,2048]{1,0:T(8,128)(2,1)} fusion(bf16[129,2048]{1,0:T(8,128)(2,1)S(1)} %concatenate.11, s32[1024]{0:T(1024)S(1)} %pad_clamp_fusion.1), kind=kCustom, calls=%fused_computation | custom fusion | bytes 4196352 | tf_op jit(solution)/shard_map/gather | solution.py:90
  33.4 54.3 %all_to_all.16 = bf16[32,1,16,2048]{3,2,1,0:T(8,128)(2,1)S(1)} all-to-all(bf16[32,1,16,2048]{3,2,1,0:T(8,128)(2,1)} %bitcast.122), channel_id=1, replica_groups=mesh['sp'=16,'tp'=2] {'sp','tp'}, dimensions={0} | all-to-all | bytes 4194304 | tf_op jit(solution)/shard_map/all_to_all | solution.py:97
  87.8 1.3 copy-done.3
  89.1 2.2 %fusion.7 = f32[512,512]{1,0:T(8,128)} fusion(bf16[512,2048]{1,0:T(8,128)(2,1)S(1)} %bitcast.124, bf16[1,2048,512]{2,1,0:T(8,128)(2,1)S(1)} %copy-done.12), kind=kOutput, calls=%fused_computation.42 | convolution fusion | flops 1073741824 | bytes 5242880 | tf_op jit(solution)/shard_map/dot_general | solution.py:99
  91.3 6.2 %convolution_convert_fusion = bf16[512,2048]{1,0:T(8,128)(2,1)} fusion(bf16[1,512,2048]{2,1,0:T(8,128)(2,1)S(1)} %copy-done, bf16[512,2048]{1,0:T(8,128)(2,1)} %bitcast.125, bf16[1,2048,512]{2,1,0:T(8,128)(2,1)} %param.29, f32[512,512]{1,0:T(8,128)} %fusion.7), kind=kOutput, calls=%fused_computation.3 | convolution fusion | flops 2150105088 | bytes 9437184 | tf_op jit(solution)/shard_map/dot_general | solution.py:102
  97.6 4.0 %all-to-all-start.2 = ((bf16[32,1,16,2048]{3,2,1,0:T(8,128)(2,1)}), bf16[32,1,16,2048]{3,2,1,0:T(8,128)(2,1)}, u32[]{:S(2)}, u32[]{:S(2)}) async-start(bf16[32,1,16,2048]{3,2,1,0:T(8,128)(2,1)} %bitcast.123), calls=%async_computation.2 | async-start | bytes 4194304 | tf_op jit(solution)/shard_map/all_to_all | solution.py:106
  101.6 2.0 %fusion.67 = f32[128,512]{1,0:T(8,128)S(1)} fusion(bf16[128,2048]{1,0:T(8,128)(2,1)S(1)} %multiply_convert_fusion, bf16[2048,512]{1,0:T(8,128)(2,1)} %param.31), kind=kOutput, calls=%fused_computation.225 | convolution fusion | flops 268435456 | bytes 2883584 | tf_op jit(solution)/shard_map/dot_general | solution.py:92
  103.7 46.6 %all-to-all-done.2 = bf16[32,1,16,2048]{3,2,1,0:T(8,128)(2,1)} async-done(((bf16[32,1,16,2048]{3,2,1,0:T(8,128)(2,1)}), bf16[32,1,16,2048]{3,2,1,0:T(8,128)(2,1)}, u32[]{:S(2)}, u32[]{:S(2)}) %all-to-all-start.2) | async-done | bytes 2097184 | tf_op jit(solution)/shard_map/all_to_all | solution.py:106
  150.2 5.2 %gather_fusion.1 = bf16[256,2048]{1,0:T(8,128)(2,1)} fusion(bf16[512,2048]{1,0:T(8,128)(2,1)} %bitcast.50, s32[1024]{0:T(1024)S(1)} %pad_clamp_fusion), kind=kCustom, calls=%fused_computation.1 | custom fusion | bytes 2098176 | tf_op jit(solution)/shard_map/gather | solution.py:109
  155.4 1.7 %reshape.135 = bf16[128,2,2048]{2,1,0:T(2,128)(2,1)S(1)} reshape(bf16[256,2048]{1,0:T(8,128)(2,1)} %gather_fusion.1) | data formatting | bytes 2097152 | tf_op jit(solution)/shard_map/reshape | solution.py:109
  157.2 2.5 %fusion.66 = (bf16[128,1,2048]{2,1,0:T(2,128)(2,1)}, bf16[128,1,2048]{2,1,0:T(2,128)(2,1)}) fusion(bf16[128,2,2048]{2,1,0:T(2,128)(2,1)S(1)} %reshape.135), kind=kLoop, calls=%fused_computation.224 | loop fusion | bytes 2097152 | tf_op jit(solution)/shard_map/slice | solution.py:114
  159.6 5.4 %fusion.3 = bf16[128,2048]{1,0:T(8,128)(2,1)} fusion(f32[128,2048]{1,0:T(8,128)} %copy-done.2, bf16[512,2048]{1,0:T(8,128)(2,1)} %param.33, bf16[128,2048]{1,0:T(8,128)(2,1)} %copy-done.1, bf16[2048,512]{1,0:T(8,128)(2,1)} %param.32, bf16[128,1,2048]{2,1,0:T(2,128)(2,1)} %get-tuple-element.8, bf16[128,1,2048]{2,1,0:T(2,128)(2,1)} %get-tuple-element.7, ...), kind=kOutput, calls=%fused_computation.38 | convolution fusion | flops 539361280 | bytes 7603200 | tf_op jit(solution)/shard_map/dot_general | solution.py:95
  (51 shorter events, 0.8 us)
Async XLA Ops:
  0.0 91.3 %copy-start = (bf16[1,512,2048]{2,1,0:T(8,128)(2,1)S(1)}, bf16[1,512,2048]{2,1,0:T(8,128)(2,1)}, u32[]{:S(2)}) copy-start(bf16[1,512,2048]{2,1,0:T(8,128)(2,1)} %param.30) | copy-start | bytes 6291460
  0.0 14.9 %copy-start.6 = (s32[256]{0:T(256)S(1)}, s32[256]{0:T(256)}, u32[]{:S(2)}) copy-start(s32[256]{0:T(256)} %param.20) | copy-start | bytes 3076
  0.0 11.7 %copy-start.5 = (bf16[31,512]{1,0:T(8,128)(2,1)S(1)}, bf16[31,512]{1,0:T(8,128)(2,1)}, u32[]{:S(2)}) copy-start(bf16[31,512]{1,0:T(8,128)(2,1)} %param.19) | copy-start | bytes 95236
  0.0 11.8 %copy-start.8 = (s32[128,2]{0,1:T(2,128)S(1)}, s32[128,2]{0,1:T(2,128)}, u32[]{:S(2)}) copy-start(s32[128,2]{0,1:T(2,128)} %param.26) | copy-start | bytes 3076
  0.9 13.9 %collective-permute-start = (s32[30]{0:T(128)S(1)}, s32[30]{0:T(128)S(1)}, u32[]{:S(2)}, u32[]{:S(2)}) collective-permute-start(s32[30]{0:T(128)S(1)} %slice.297), channel_id=1, source_target_pairs={{0,2},{2,4},{4,6},{6,8},{8,10},{10,12},{12,14},{14,16},{16,18},{18... | collective-permute-start | bytes 368 | tf_op jit(solution)/shard_map/ppermute | solution.py:13
  6.9 14.7 %copy-start.9 = (f32[512]{0:T(512)S(1)}, f32[512]{0:T(512)}, u32[]{:S(2)}) copy-start(f32[512]{0:T(512)} %param.22) | copy-start | bytes 6148
  6.9 14.7 %copy-start.10 = (f32[512]{0:T(512)S(1)}, f32[512]{0:T(512)}, u32[]{:S(2)}) copy-start(f32[512]{0:T(512)} %param.21) | copy-start | bytes 6148
  8.3 6.9 %collective-permute-start.1 = (bf16[30,512]{0,1:T(8,128)(2,1)S(1)}, bf16[30,512]{0,1:T(8,128)(2,1)S(1)}, u32[]{:S(2)}, u32[]{:S(2)}) collective-permute-start(bf16[30,512]{0,1:T(8,128)(2,1)S(1)} %slice.400), channel_id=1, source_target_pairs={{0,2},{2,4},{4,6},{6,8},{8,10},{10,12},{12,14},{14,16},{16,18},{18... | collective-permute-start | bytes 92168 | tf_op jit(solution)/shard_map/ppermute | solution.py:13
  13.4 12.5 %copy-start.4 = (bf16[128,2048]{1,0:T(8,128)(2,1)S(1)}, bf16[128,2048]{1,0:T(8,128)(2,1)}, u32[]{:S(2)}) copy-start(bf16[128,2048]{1,0:T(8,128)(2,1)} %param.24) | copy-start | bytes 1572868
  25.9 4.0 %copy-start.7 = (f32[2048]{0:T(1024)S(1)}, f32[2048]{0:T(1024)}, u32[]{:S(2)}) copy-start(f32[2048]{0:T(1024)} %param.25) | copy-start | bytes 24580
  28.9 1.0 copy-start.2
  30.0 71.6 %copy-start.1 = (bf16[128,2048]{1,0:T(8,128)(2,1)}, bf16[128,2048]{1,0:T(8,128)(2,1)S(1)}, u32[]{:S(2)}) copy-start(bf16[128,2048]{1,0:T(8,128)(2,1)S(1)} %multiply_convert_fusion) | copy-start | bytes 1572868
  33.4 55.7 %copy-start.12 = (bf16[1,2048,512]{2,1,0:T(8,128)(2,1)S(1)}, bf16[1,2048,512]{2,1,0:T(8,128)(2,1)}, u32[]{:S(2)}) copy-start(bf16[1,2048,512]{2,1,0:T(8,128)(2,1)} %param.28) | copy-start | bytes 6291460
  87.8 1.3 copy-start.3
  97.6 4.0 %copy-start.11 = (f32[128,2]{0,1:T(2,128)S(1)}, f32[128,2]{0,1:T(2,128)}, u32[]{:S(2)}) copy-start(f32[128,2]{0,1:T(2,128)} %param.27) | copy-start | bytes 3076
  97.6 52.6 %all-to-all-start.2 = ((bf16[32,1,16,2048]{3,2,1,0:T(8,128)(2,1)}), bf16[32,1,16,2048]{3,2,1,0:T(8,128)(2,1)}, u32[]{:S(2)}, u32[]{:S(2)}) async-start(bf16[32,1,16,2048]{3,2,1,0:T(8,128)(2,1)} %bitcast.123), calls=%async_computation.2 | async-start | bytes 4194304 | tf_op jit(solution)/shard_map/all_to_all | solution.py:106
